TPU v7x, 32 devices: a whole 2x2x4 slice. The times are simulated.
32 devices in a mesh: sp: 8 (over z, x), tp: 4 (over y, core).
Axes of the slice: x: 2, y: 2, z: 4, core: 2. Of those that a mesh axis runs over, the one named last changes fastest.
Arguments:
- wide_query: bfloat16 [4096, 1536], P('sp', 'tp'), may hold values from -6 to 6
- wide_key: bfloat16 [4096, 1536], P('sp', 'tp'), may hold values from -6 to 6
- wide_value: bfloat16 [4096, 1536], P('sp', 'tp'), may hold values from -6 to 6
- wide_gate: bfloat16 [4096, 1536], P('sp', 'tp'), may hold values from -6 to 6
- narrow_query: bfloat16 [4096, 512], P('sp', 'tp'), may hold values from -6 to 6
- narrow_key: bfloat16 [4096, 512], P('sp', 'tp'), may hold values from -6 to 6
- narrow_value: bfloat16 [4096, 512], P('sp', 'tp'), may hold values from -6 to 6
- narrow_gate: bfloat16 [4096, 512], P('sp', 'tp'), may hold values from -6 to 6
- wide_decay: float32 [12, 4096], P('tp', 'sp'), may hold values from -1 to 0
- narrow_decay: float32 [8, 4096], P('tp', 'sp'), may hold values from -1 to 0
- residual: bfloat16 [4096, 2048], P(('sp', 'tp')), may hold values from -6 to 6
- wide_out: bfloat16 [1536, 2048], P('tp'), may hold values from -0.125 to 0.125
- narrow_out: bfloat16 [512, 2048], P('tp'), may hold values from -0.125 to 0.125
- up_weight: bfloat16 [2048, 8192], P('sp', 'tp'), may hold values from -0.125 to 0.125
- down_weight: bfloat16 [8192, 2048], P('tp', 'sp'), may hold values from -0.0625 to 0.0625
- gain_mix: float32 [2048], replicated, may hold values from 0.1 to 1.9
- gain_pre: float32 [2048], replicated, may hold values from 0.1 to 1.9
- gain_mlp: float32 [2048], replicated, may hold values from 0.1 to 1.9
Outputs:
- result: bfloat16 [4096, 2048], P(('sp', 'tp'))
All inputs are finite; a program needn't handle non-finite values.
Results may differ from a plain program's by a relative error of at most 0.02.
Values may be sent and summed in bfloat16 or wider, within the bound.
A program may use at most 128 MiB of HBM per device.

v0:
```python
import jax
import jax.numpy as jnp
from jax import lax
from jax.sharding import PartitionSpec as P

WIDE_DIM = 128
NARROW_DIM = 64
SPAN = 128
epsilon = 1e-06


def prefix_2(array, axis, join, neutral):
    place = lax.axis_index(axis)
    gathered = jax.tree.map(
        lambda a, kind: lax.all_gather(a.astype(kind), axis),
        array,
        (jnp.bfloat16, jnp.bfloat16, jnp.bfloat16, jnp.bfloat16),
    )
    state = jax.tree.map(lambda a, e: jnp.zeros_like(a) + jnp.asarray(e, a.dtype), array, neutral)

    def one(turn, state):
        return join(
            state,
            jax.tree.map(
                lambda a, own: lax.dynamic_index_in_dim(a, turn, 0, False).astype(own.dtype),
                gathered,
                array,
            ),
        )

    return lax.fori_loop(0, place, one, state)


def rotate(packed, head_dim, positions):
    length = packed.shape[0]
    grouped = packed.astype(jnp.float32).reshape(length, -1, head_dim)
    halfway = head_dim // 2
    inverse = 10000.0 ** (-jnp.arange(0, head_dim, 2, dtype=jnp.float32) / head_dim)
    angles = positions.astype(jnp.float32)[:, None] * inverse[None, :]
    cosine_table = jnp.cos(angles)[:, None, :]
    sine_table = jnp.sin(angles)[:, None, :]
    leading = grouped[..., :halfway]
    trailing = grouped[..., halfway:]
    return jnp.concatenate(
        [
            leading * cosine_table - trailing * sine_table,
            leading * sine_table + trailing * cosine_table,
        ],
        axis=-1,
    )


def rms_scale(values, gain_vector):
    return (
        values
        * lax.rsqrt(jnp.mean(values * values, axis=-1, keepdims=True) + epsilon)
        * gain_vector
    )


def span_terms(query, key, value, log_decay, head_dim, offset):
    length = query.shape[0]
    count_of_heads = query.shape[1] // head_dim
    span_count = length // SPAN
    shaped = (span_count, SPAN, count_of_heads, head_dim)
    positions = offset + jnp.arange(length, dtype=jnp.int32)
    queries = rotate(query, head_dim, positions).astype(jnp.bfloat16).reshape(shaped)
    keys_full = (rotate(key, head_dim, positions) * head_dim ** (-0.5)).reshape(shaped)
    keys_half = keys_full.astype(jnp.bfloat16)
    values_all = value.reshape(shaped)
    cumulative = jnp.cumsum(log_decay.T.reshape(span_count, SPAN, count_of_heads), axis=1)
    causal = jnp.arange(SPAN)[:, None] >= jnp.arange(SPAN)[None, :]
    scores = jnp.einsum("nihd,njhd->nhij", queries, keys_half, preferred_element_type=jnp.float32)
    decay_rows = cumulative.transpose(0, 2, 1)
    log_gaps = jnp.where(causal, decay_rows[..., :, None] - decay_rows[..., None, :], -jnp.inf)
    weights = (scores * jnp.exp(log_gaps)).astype(jnp.bfloat16)
    within = jnp.einsum("nhij,njhd->nihd", weights, values_all, preferred_element_type=jnp.float32)
    span_total = cumulative[:, -1, :]
    scaled = (keys_full * jnp.exp(span_total[:, None, :] - cumulative)[..., None]).astype(
        jnp.bfloat16
    )
    own_state = jnp.einsum(
        "njhd,njhe->nhde", scaled, values_all, preferred_element_type=jnp.float32
    )

    def advance(carried, inputs):
        decay_sum, contribution = inputs
        return (carried * jnp.exp(decay_sum)[:, None, None] + contribution, carried)

    initial = jnp.zeros((count_of_heads, head_dim, head_dim), jnp.float32)
    closing, before = lax.scan(advance, initial, (span_total, own_state))
    device_decay = jnp.exp(jnp.sum(span_total, axis=0))
    return (queries, cumulative, within, span_total, before, closing, device_decay)


def finish(parts, prefix, gate, head_dim):
    queries, cumulative, within, span_total, before, closing, device_decay = parts
    length = gate.shape[0]
    earlier = jnp.cumsum(span_total, axis=0) - span_total
    entering = (prefix[None] * jnp.exp(earlier)[:, :, None, None] + before).astype(jnp.bfloat16)
    across = (
        jnp.einsum("nihd,nhde->nihe", queries, entering, preferred_element_type=jnp.float32)
        * jnp.exp(cumulative)[..., None]
    )
    output = (within + across).reshape(length, -1, head_dim)
    normed = output * lax.rsqrt(jnp.mean(output * output, axis=-1, keepdims=True) + epsilon)
    return (normed.reshape(length, -1) * jax.nn.silu(gate.astype(jnp.float32))).astype(jnp.bfloat16)


def combine_states(former, latter):
    return (
        former[0] * latter[0],
        former[1] * latter[0][:, None, None] + latter[1],
        former[2] * latter[2],
        former[3] * latter[2][:, None, None] + latter[3],
    )


def local(
    wide_query,
    wide_key,
    wide_value,
    wide_gate,
    narrow_query,
    narrow_key,
    narrow_value,
    narrow_gate,
    wide_decay,
    narrow_decay,
    residual,
    wide_out,
    narrow_out,
    up_weight,
    down_weight,
    gain_mix,
    gain_pre,
    gain_mlp,
):
    length = wide_query.shape[0]
    offset = lax.axis_index("sp") * length
    wide_parts = span_terms(wide_query, wide_key, wide_value, wide_decay, WIDE_DIM, offset)
    narrow_parts = span_terms(
        narrow_query, narrow_key, narrow_value, narrow_decay, NARROW_DIM, offset
    )
    identity = (
        jnp.ones_like(wide_parts[6]),
        jnp.zeros_like(wide_parts[5]),
        jnp.ones_like(narrow_parts[6]),
        jnp.zeros_like(narrow_parts[5]),
    )
    prefixes = prefix_2(
        (wide_parts[6], wide_parts[5], narrow_parts[6], narrow_parts[5]),
        "sp",
        combine_states,
        identity,
    )
    wide_mixed = finish(wide_parts, prefixes[1], wide_gate, WIDE_DIM)
    narrow_mixed = finish(narrow_parts, prefixes[3], narrow_gate, NARROW_DIM)
    wide_rows, narrow_rows = (
        lax.all_to_all(wide_mixed, "tp", split_axis=0, concat_axis=1, tiled=True),
        lax.all_to_all(narrow_mixed, "tp", split_axis=0, concat_axis=1, tiled=True),
    )
    wide_whole, narrow_whole = (
        lax.all_gather(wide_out, "tp", axis=0, tiled=True),
        lax.all_gather(narrow_out, "tp", axis=0, tiled=True),
    )
    projected = jnp.dot(wide_rows, wide_whole, preferred_element_type=jnp.float32) + jnp.dot(
        narrow_rows, narrow_whole, preferred_element_type=jnp.float32
    )
    updated = (residual.astype(jnp.float32) + rms_scale(projected, gain_mix)).astype(jnp.bfloat16)
    normed = rms_scale(updated.astype(jnp.float32), gain_pre).astype(jnp.bfloat16)
    block_rows = lax.all_gather(normed, "tp", axis=0, tiled=True)
    rectified = jax.nn.relu(
        jnp.dot(
            block_rows,
            lax.all_gather(up_weight, "sp", axis=0, tiled=True),
            preferred_element_type=jnp.float32,
        )
    )
    hidden = (rectified * rectified).astype(jnp.bfloat16)
    partial_terms = jnp.dot(
        hidden,
        lax.all_gather(down_weight, "sp", axis=1, tiled=True),
        preferred_element_type=jnp.float32,
    )
    lowered = lax.psum_scatter(
        partial_terms.astype(jnp.bfloat16), "tp", scatter_dimension=0, tiled=True
    ).astype(jnp.float32)
    return (updated.astype(jnp.float32) + rms_scale(lowered, gain_mlp)).astype(jnp.bfloat16)


def solution(mesh):
    return jax.shard_map(
        local,
        mesh=mesh,
        in_specs=(
            P("sp", "tp"),
            P("sp", "tp"),
            P("sp", "tp"),
            P("sp", "tp"),
            P("sp", "tp"),
            P("sp", "tp"),
            P("sp", "tp"),
            P("sp", "tp"),
            P("tp", "sp"),
            P("tp", "sp"),
            P(("sp", "tp"), None),
            P("tp", None),
            P("tp", None),
            P("sp", "tp"),
            P("tp", "sp"),
            P(),
            P(),
            P(),
        ),
        out_specs=P(("sp", "tp"), None),
        check_vma=False,
    )
```

profile of v0, /device:TPU:0, one launch (start us, length us, event | category | flops | bytes accessed | tf_op | source)
XLA Modules:
  0.0 507.7 jit_solution(15633803309684791243)
XLA Ops:
  8.1 1.2 copy.77
  14.4 3.3 while.42
  17.7 33.8 %all-gather.1 = bf16[24,128,128]{2,1,0:T(8,128)(2,1)S(1)} all-gather(bf16[3,128,128]{2,1,0:T(8,128)(2,1)S(1)} %convert_element_type.154), channel_id=3, replica_groups=mesh['sp'=8,'tp'=4] {'sp'}, dimensions={0}, use_global_device_ids=true | all-gather | bytes 884736 | tf_op jit(solution)/shard_map/all_gather | solution.py:15
  52.5 1.7 copy.93
  55.1 1.7 copy.106
  57.8 1.6 fusion.61
  61.0 1.2 reduce_window_sum.45
  65.0 1.8 reshape.384
  66.7 1.7 copy.99
  68.5 1.6 bitcast_dynamic-update-slice_fusion.2
  70.0 1.9 fusion.54
  71.9 6.2 %while.43 = (s32[]{:T(128)}, f32[2,64,64]{2,1,0:T(8,128)S(1)}, f32[4,2,64,64]{3,2,1,0:T(8,128)}, f32[4,2]{1,0:T(4,128)S(1)}, f32[4,2,64,64]{3,2,1,0:T(8,128)}, /*index=5*/s32[]{:T(128)}, s32[]{:T(128)}) while((s32[]{:T(128)}, f32[2,64,64]{2,1,0:T(8,128)S(1)}, f32[4,2,64,64]{3,2,1,0:T(8,128)}, f32[4,2]{1,0:T(4,128)S(1)}, ...), condition=%wide.region_7.8_spmd.clone, body=%wide.region_6.7_spmd.clone.sunk | while | flops 32771 | bytes 197240 | solution.py:91
  78.1 32.7 %all-gather.3 = bf16[16,64,64]{2,1,0:T(8,128)(2,1)} all-gather(bf16[2,64,64]{2,1,0:T(8,128)(2,1)S(1)} %convert_element_type.158), channel_id=5, replica_groups=mesh['sp'=8,'tp'=4] {'sp'}, dimensions={0}, use_global_device_ids=true | all-gather | bytes 147456 | tf_op jit(solution)/shard_map/all_gather | solution.py:15
  111.6 1.3 dynamic-slice
  114.6 21.4 %all-reduce.2 = (bf16[24]{0:T(256)(128)(2,1)S(1)}, bf16[16]{0:T(256)(128)(2,1)S(1)}) all-reduce(bf16[24]{0:T(256)(128)(2,1)S(1)} %dynamic-update-slice, bf16[16]{0:T(256)(128)(2,1)S(1)} %dynamic-update-slice.1), channel_id=2, replica_groups=mesh['sp'=8,'tp'=4] {'sp'}, use_global_device_ids=true, to_apply=%add | all-reduce | flops 40 | bytes 160
  137.5 1.7 concatenate.35
  139.1 1.2 copy.79
  142.1 2.6 fusion.8
  144.7 3.1 multiply_reduce_fusion.1
  147.8 1.7 copy.103
  151.8 3.5 all-to-all-start
  157.8 4.8 all-to-all-done
  162.7 3.3 all-to-all-start.1
  166.3 3.8 fusion.77
  170.6 2.1 multiply_reduce_fusion
  175.4 24.6 %all-gather.14.cloned.1.call-done = bf16[512,2048]{1,0:T(8,128)(2,1)} async-done(((bf16[128,2048]{1,0:T(8,128)(2,1)}), bf16[512,2048]{1,0:T(8,128)(2,1)}) %all-gather.14.cloned.1.call-update) | async-done | bytes 2097168 | tf_op jit(solution)/shard_map/all_gather | solution.py:172
  200.0 126.5 %all-gather.16.cloned.1.call-done = bf16[2048,2048]{1,0:T(8,128)(2,1)} async-done(((bf16[256,2048]{1,0:T(8,128)(2,1)}), bf16[2048,2048]{1,0:T(8,128)(2,1)}) %all-gather.16.cloned.1.call-update) | async-done | bytes 8388624 | tf_op jit(solution)/shard_map/all_gather | solution.py:176
  326.4 125.0 %all-gather.18.cloned.1.call-done = bf16[2048,2048]{1,0:T(8,128)(2,1)} async-done(((bf16[2048,256]{1,0:T(8,128)(2,1)}), bf16[2048,2048]{1,0:T(8,128)(2,1)}) %all-gather.18.cloned.1.call-update) | async-done | bytes 8388624 | tf_op jit(solution)/shard_map/all_gather | solution.py:183
  451.5 16.5 %convolution_convert_fusion = bf16[512,2048]{1,0:T(8,128)(2,1)} fusion(bf16[2048,2048]{1,0:T(8,128)(2,1)} %all-gather.18.cloned.1.call-done, bf16[512,2048]{1,0:T(8,128)(2,1)} %all-gather.14.cloned.1.call-done, bf16[2048,2048]{1,0:T(8,128)(2,1)} %all-gather.16.cloned.1.call-done), kind=kOutput, calls=%fused_computation.19 | convolution fusion | flops 8594128896 | bytes 20971520 | tf_op jit(solution)/shard_map/dot_general | solution.py:181
  468.0 29.5 %reduce-scatter.2.cloned.1.call-done = bf16[128,2048]{1,0:T(8,128)(2,1)} async-done(((bf16[512,2048]{1,0:T(8,128)(2,1)}), bf16[128,2048]{1,0:T(8,128)(2,1)}) %reduce-scatter.2.cloned.1.call-update) | async-done | bytes 524304 | tf_op jit(solution)/shard_map/reduce_scatter | solution.py:186
  497.5 1.2 fusion.16
  498.8 2.1 fusion.21
  (153 shorter events, 35.6 us)
Async XLA Ops:
  6.5 2.8 copy-start.7
  6.5 159.7 %all-gather.10.cloned.1.call-start = ((), (), s32[]{:S(2)}) async-start(), calls=%async_computation.3 | async-start | bytes 7864320 | tf_op jit(solution)/shard_map/all_gather | solution.py:164
  7.3 163.3 %all-gather.12.cloned.1.call-start = ((), (), s32[]{:S(2)}) async-start(), calls=%async_computation.4 | async-start | bytes 2621440 | tf_op jit(solution)/shard_map/all_gather | solution.py:165
  9.6 2.5 copy-start.17
  10.2 3.2 copy-start.6
  14.4 45.7 %copy-start.18 = (f32[2,512]{1,0:T(2,128)S(1)}, f32[2,512]{1,0:T(2,128)}, u32[]{:S(2)}) copy-start(f32[2,512]{1,0:T(2,128)} %param.33) | copy-start | bytes 12292
  62.2 74.0 %copy-start = (f32[4,128,2]{2,1,0:T(8,128)}, f32[4,128,2]{2,1,0:T(8,128)S(1)}, u32[]{:S(2)}) copy-start(f32[4,128,2]{2,1,0:T(8,128)S(1)} %reduce_window_sum.45) | copy-start | bytes 12292
  62.9 1.0 copy-start.12
  144.7 11.0 %copy-start.1 = (f32[4,128,2]{2,1,0:T(8,128)S(1)}, f32[4,128,2]{2,1,0:T(8,128)}, u32[]{:S(2)}) copy-start(f32[4,128,2]{2,1,0:T(8,128)} %copy-done) | copy-start | bytes 12292
  144.7 11.1 %copy-start.8 = (bf16[2,4,4,8,128]{4,3,2,1,0:T(8,128)(2,1)S(1)}, bf16[2,4,4,8,128]{4,3,2,1,0:T(8,128)(2,1)}, u32[]{:S(2)}) copy-start(bf16[2,4,4,8,128]{4,3,2,1,0:T(8,128)(2,1)} %get-tuple-element.233) | copy-start | bytes 196612
  147.8 7.5 %copy-start.13 = (f32[4,1,2]{0,2,1:T(2,128)S(1)}, f32[4,1,2]{0,2,1:T(2,128)}, u32[]{:S(2)}) copy-start(f32[4,1,2]{0,2,1:T(2,128)} %copy-done.12) | copy-start | bytes 100
  147.8 7.7 %copy-start.2 = (f32[4,128,2]{2,1,0:T(8,128)S(1)}, f32[4,128,2]{2,1,0:T(8,128)}, u32[]{:S(2)}) copy-start(f32[4,128,2]{2,1,0:T(8,128)} %get-tuple-element.236) | copy-start | bytes 12292
  147.8 8.1 %copy-start.9 = (f32[4,2,64,64]{3,2,1,0:T(8,128)S(1)}, f32[4,2,64,64]{3,2,1,0:T(8,128)}, u32[]{:S(2)}) copy-start(f32[4,2,64,64]{3,2,1,0:T(8,128)} %get-tuple-element.136) | copy-start | bytes 393220
  147.8 8.4 %copy-start.3 = (f32[4,128,2,64]{1,3,2,0:T(8,128)S(1)}, f32[4,128,2,64]{1,3,2,0:T(8,128)}, u32[]{:S(2)}) copy-start(f32[4,128,2,64]{1,3,2,0:T(8,128)} %bitcast_dynamic-update-slice_fusion.2) | copy-start | bytes 786436
  147.8 8.4 %copy-start.4 = (bf16[4,128,2,64]{1,3,2,0:T(8,128)(2,1)S(1)}, bf16[4,128,2,64]{1,3,2,0:T(8,128)(2,1)}, u32[]{:S(2)}) copy-start(bf16[4,128,2,64]{1,3,2,0:T(8,128)(2,1)} %copy.99) | copy-start | bytes 393220
  147.8 8.4 %copy-start.11 = (pred[128,128]{1,0:T(8,128)(4,1)S(1)}, pred[128,128]{1,0:T(8,128)(4,1)}, u32[]{:S(2)}) copy-start(pred[128,128]{1,0:T(8,128)(4,1)} %iota_compare_fusion) | copy-start | bytes 49156
  147.8 9.1 %copy-start.10 = (bf16[512,128]{1,0:T(8,128)(2,1)S(1)}, bf16[512,128]{1,0:T(8,128)(2,1)}, u32[]{:S(2)}) copy-start(bf16[512,128]{1,0:T(8,128)(2,1)} %param.31) | copy-start | bytes 393220
  151.8 10.8 %all-to-all-start = ((bf16[4,128,384]{1,2,0:T(8,128)(2,1)}), bf16[4,128,384]{1,2,0:T(8,128)(2,1)S(1)}, u32[]{:S(2)}, u32[]{:S(2)}) async-start(bf16[4,128,384]{1,2,0:T(8,128)(2,1)} %copy_bitcast_fusion), calls=%async_computation | async-start | bytes 786432 | tf_op jit(solution)/shard_map/all_to_all | solution.py:160
  162.7 7.9 %all-to-all-start.1 = ((bf16[4,128,128]{1,2,0:T(8,128)(2,1)}), bf16[4,128,128]{1,2,0:T(8,128)(2,1)S(1)}, u32[]{:S(2)}, u32[]{:S(2)}) async-start(bf16[4,128,128]{1,2,0:T(8,128)(2,1)} %copy_bitcast_fusion.1), calls=%async_computation.1 | async-start | bytes 262144 | tf_op jit(solution)/shard_map/all_to_all | solution.py:161
  166.0 34.0 %all-gather.14.cloned.1.call-start = ((), (), s32[]{:S(2)}) async-start(), calls=%async_computation.5 | async-start | bytes 2621440 | tf_op jit(solution)/shard_map/all_gather | solution.py:172
  170.1 2.7 copy-start.5
  170.1 2.7 copy-start.14
  170.1 3.0 copy-start.15
  174.1 152.3 %all-gather.16.cloned.1.call-start = ((), (), s32[]{:S(2)}) async-start(), calls=%async_computation.6 | async-start | bytes 9437184 | tf_op jit(solution)/shard_map/all_gather | solution.py:176
  174.7 276.8 %all-gather.18.cloned.1.call-start = ((), (), s32[]{:S(2)}) async-start(), calls=%async_computation.7 | async-start | bytes 9437184 | tf_op jit(solution)/shard_map/all_gather | solution.py:183
  175.3 323.5 %copy-start.16 = (f32[2048]{0:T(1024)S(1)}, f32[2048]{0:T(1024)}, u32[]{:S(2)}) copy-start(f32[2048]{0:T(1024)} %param.41) | copy-start | bytes 24580
  175.3 322.2 %reduce-scatter.2.cloned.1.call-start = ((), (), s32[]{:S(2)}) async-start(), calls=%async_computation.8 | async-start | bytes 2621440 | tf_op jit(solution)/shard_map/reduce_scatter | solution.py:186
Sparse Core Ops, SparseCore 0:
  8.9 49.0 all-gather.9
  59.6 22.5 all-gather.11
  174.3 25.6 all-gather.13
  201.9 124.4 all-gather.15
  328.3 123.1 all-gather.17
  468.1 29.3 reduce-scatter.1
where the time goes:
time: 509 us; the launch traced here: 508 us
  waiting for transfers between devices  313 us (61%)
  blocking collectives  88 us (17%)
  matrix products  31.6 us (6%)
  local copies, waits for them, and re-layouts  26.2 us (5%)
  other arithmetic  26.1 us (5%)
  between operations  15.2 us (3%)
  starting transfers between devices  7.16 us (1%)
    all_gather x1, waiting for transfers between devices, local(): lax.all_gather(up_weight, 'sp', axis=0, tiled=True)  126 us
    all_gather x1, waiting for transfers between devices, local(): lax.all_gather(down_weight, 'sp', axis=1, tiled=True)  125 us
    all_gather x2, blocking collectives, prefix_2(): lax.all_gather(a.astype(kind), axis)  66.6 us
    reduce_scatter x1, waiting for transfers between devices, local(): lax.psum_scatter(partial_terms.astype(jnp.bfloat16), 'tp', scatter_dimens...  29.5 us
    all_gather x1, waiting for transfers between devices, local(): block_rows = lax.all_gather(normed, 'tp', axis=0, tiled=True)  24.6 us
    unnamed x1, blocking collectives  21.4 us
    dot_general x1, matrix products, local(): jnp.dot(hidden, lax.all_gather(down_weight, 'sp', axis=1, tiled=True), pr...  16.5 us
  transfers between devices with their start and end apart: 8, of which 6 were waited for; matrix products, arithmetic and copies ran while one was open for 12% of the time, Pallas kernels for 0%

commit v1 on v0

--- a/solution.py
+++ b/solution.py
@@ -180,7 +180,9 @@
     hidden = (rectified * rectified).astype(jnp.bfloat16)
     partial_terms = jnp.dot(
         hidden,
-        lax.all_gather(down_weight, "sp", axis=1, tiled=True),
+        jnp.concatenate(
+            lax.all_to_all(jnp.stack([down_weight] * lax.axis_size("sp")), "sp", 0, 0), axis=1
+        ),
         preferred_element_type=jnp.float32,
     )
     lowered = lax.psum_scatter(

time: 509 us -> 515 us (1.012)
  starting transfers between devices: 7.16 us -> 15.9 us
  other arithmetic: 26.1 us -> 18 us
  waiting for transfers between devices: 313 us -> 321 us
    all_to_all x0 -> x1, waiting for transfers between devices: none -> 271 us  [local(): lax.all_to_all(jnp.stack([down_weight] * lax.axis_size('sp')), 'sp', 0, 0)]
    all_gather x1, waiting for transfers between devices: 126 us -> 0.01 us  [local(): lax.all_gather(up_weight, 'sp', axis=0, tiled=True)]
    all_gather x1 -> x0, waiting for transfers between devices: 125 us -> none  [local(): lax.all_gather(down_weight, 'sp', axis=1, tiled=True)]
    all_gather x1, waiting for transfers between devices: 24.6 us -> 12.5 us  [local(): block_rows = lax.all_gather(normed, 'tp', axis=0, tiled=True)]
    all_to_all x0 -> x1, starting transfers between devices: none -> 8.76 us  [local(): lax.all_to_all(jnp.stack([down_weight] * lax.axis_size('sp')), 'sp', 0, 0)]
  transfers between devices with their start and end apart: 8 -> 8, of which waited for: 6 -> 5; matrix products, arithmetic and copies ran while one was open for 12% -> 10% of each run, Pallas kernels for 0% -> 0%
where the time goes in v1:
time: 515 us; the launch traced here: 514 us
  waiting for transfers between devices  321 us (62%)
  blocking collectives  87.9 us (17%)
  matrix products  31 us (6%)
  local copies, waits for them, and re-layouts  24.6 us (5%)
  other arithmetic  18 us (3%)
  starting transfers between devices  15.9 us (3%)
  between operations  15.1 us (3%)
    all_to_all x1, waiting for transfers between devices, local(): lax.all_to_all(jnp.stack([down_weight] * lax.axis_size('sp')), 'sp', 0, 0)  271 us
    all_gather x2, blocking collectives, prefix_2(): lax.all_gather(a.astype(kind), axis)  66.8 us
    reduce_scatter x1, waiting for transfers between devices, local(): lax.psum_scatter(partial_terms.astype(jnp.bfloat16), 'tp', scatter_dimens...  30.3 us
    unnamed x1, blocking collectives  21.1 us
    dot_general x1, matrix products, local(): jnp.dot(hidden, jnp.concatenate(lax.all_to_all(jnp.stack([down_weight] *...  16.5 us
    all_gather x1, waiting for transfers between devices, local(): block_rows = lax.all_gather(normed, 'tp', axis=0, tiled=True)  12.5 us
  transfers between devices with their start and end apart: 8, of which 5 were waited for; matrix products, arithmetic and copies ran while one was open for 10% of the time, Pallas kernels for 0%

profile of v1, /device:TPU:0, one launch (start us, length us, event | category | flops | bytes accessed | tf_op | source)
XLA Modules:
  0.0 514.1 jit_solution(6921613934496432781)
XLA Ops:
  8.1 1.2 copy.78
  10.2 1.0 subtract_convert_fusion
  14.9 3.2 while.42
  18.2 36.0 %all-gather.1 = bf16[24,128,128]{2,1,0:T(8,128)(2,1)} all-gather(bf16[3,128,128]{2,1,0:T(8,128)(2,1)S(1)} %convert_element_type.154), channel_id=3, replica_groups=mesh['sp'=8,'tp'=4] {'sp'}, dimensions={0}, use_global_device_ids=true | all-gather | bytes 884736 | tf_op jit(solution)/shard_map/all_gather | solution.py:15
  54.5 1.0 copy.94
  55.6 1.0 copy.107
  60.5 1.6 bitcast_dynamic-update-slice_fusion.2
  62.1 1.1 fusion.54
  63.2 2.9 while.43
  66.1 30.8 %all-gather.3 = bf16[16,64,64]{2,1,0:T(8,128)(2,1)S(1)} all-gather(bf16[2,64,64]{2,1,0:T(8,128)(2,1)S(1)} %convert_element_type.158), channel_id=5, replica_groups=mesh['sp'=8,'tp'=4] {'sp'}, dimensions={0}, use_global_device_ids=true | all-gather | bytes 147456 | tf_op jit(solution)/shard_map/all_gather | solution.py:15
  99.4 21.1 %all-reduce.2 = (bf16[24]{0:T(256)(128)(2,1)S(1)}, bf16[16]{0:T(256)(128)(2,1)S(1)}) all-reduce(bf16[24]{0:T(256)(128)(2,1)S(1)} %dynamic-update-slice, bf16[16]{0:T(256)(128)(2,1)S(1)} %dynamic-update-slice.1), channel_id=2, replica_groups=mesh['sp'=8,'tp'=4] {'sp'}, use_global_device_ids=true, to_apply=%add | all-reduce | flops 40 | bytes 160
  121.5 1.2 copy.79
  123.4 1.2 copy.80
  125.1 1.1 copy.103
  126.9 2.7 fusion.8
  129.6 3.1 multiply_reduce_fusion.1
  132.8 1.7 copy.104
  134.5 1.2 copy.105
  136.8 3.5 all-to-all-start
  142.8 4.9 all-to-all-done
  147.7 3.3 all-to-all-start.1
  151.2 3.8 fusion.77
  155.6 2.1 multiply_reduce_fusion
  158.1 1.0 fusion.20
  159.8 4.3 stack.2
  164.1 8.8 %all-to-all-start.2 = ((bf16[8,2048,256]{1,2,0:T(8,128)(2,1)}), bf16[8,2048,256]{1,2,0:T(8,128)(2,1)}, u32[]{:S(2)}, u32[]{:S(2)}) async-start(bf16[8,2048,256]{1,2,0:T(8,128)(2,1)} %stack.2), calls=%async_computation.2 | async-start | bytes 16777216 | tf_op jit(solution)/shard_map/all_to_all | solution.py:184
  173.5 12.5 %all-gather.13.cloned.1.call-done = bf16[512,2048]{1,0:T(8,128)(2,1)} async-done(((bf16[128,2048]{1,0:T(8,128)(2,1)}), bf16[512,2048]{1,0:T(8,128)(2,1)}) %all-gather.13.cloned.1.call-update) | async-done | bytes 2097168 | tf_op jit(solution)/shard_map/all_gather | solution.py:172
  185.9 271.4 %all-to-all-done.2 = bf16[8,2048,256]{1,2,0:T(8,128)(2,1)} async-done(((bf16[8,2048,256]{1,2,0:T(8,128)(2,1)}), bf16[8,2048,256]{1,2,0:T(8,128)(2,1)}, u32[]{:S(2)}, u32[]{:S(2)}) %all-to-all-start.2) | async-done | bytes 8388640 | tf_op jit(solution)/shard_map/all_to_all | solution.py:184
  457.4 16.5 %convolution_convert_fusion = bf16[512,2048]{1,0:T(8,128)(2,1)} fusion(bf16[2048,2048]{0,1:T(8,128)(2,1)} %bitcast.37, bf16[512,2048]{1,0:T(8,128)(2,1)} %all-gather.13.cloned.1.call-done, bf16[2048,2048]{1,0:T(8,128)(2,1)} %all-gather.15.cloned.1.call-done), kind=kOutput, calls=%fused_computation.19 | convolution fusion | flops 8594128896 | bytes 20971520 | tf_op jit(solution)/shard_map/dot_general | solution.py:181
  473.9 30.3 %reduce-scatter.2.cloned.1.call-done = bf16[128,2048]{1,0:T(8,128)(2,1)} async-done(((bf16[512,2048]{1,0:T(8,128)(2,1)}), bf16[128,2048]{1,0:T(8,128)(2,1)}) %reduce-scatter.2.cloned.1.call-update) | async-done | bytes 524304 | tf_op jit(solution)/shard_map/reduce_scatter | solution.py:188
  504.2 1.2 fusion.16
  505.5 2.1 fusion.21
  (166 shorter events, 26.3 us)
Async XLA Ops:
  6.5 2.8 copy-start.9
  6.5 144.7 %all-gather.9.cloned.1.call-start = ((), (), s32[]{:S(2)}) async-start(), calls=%async_computation.4 | async-start | bytes 7864320 | tf_op jit(solution)/shard_map/all_gather | solution.py:164
  7.3 148.3 %all-gather.11.cloned.1.call-start = ((), (), s32[]{:S(2)}) async-start(), calls=%async_computation.5 | async-start | bytes 2621440 | tf_op jit(solution)/shard_map/all_gather | solution.py:165
  9.6 2.5 copy-start.21
  10.2 3.8 copy-start.8
  14.9 43.2 %copy-start.22 = (f32[2,512]{1,0:T(2,128)S(1)}, f32[2,512]{1,0:T(2,128)}, u32[]{:S(2)}) copy-start(f32[2,512]{1,0:T(2,128)} %param.33) | copy-start | bytes 12292
  14.9 45.2 %copy-start.13 = (bf16[512,128]{1,0:T(8,128)(2,1)S(1)}, bf16[512,128]{1,0:T(8,128)(2,1)}, u32[]{:S(2)}) copy-start(bf16[512,128]{1,0:T(8,128)(2,1)} %param.30) | copy-start | bytes 393220
  54.5 42.4 %copy-start.23 = (f32[3]{0:T(128)S(1)}, f32[3]{0:T(128)}, u32[]{:S(2)}) copy-start(f32[3]{0:T(128)} %get-tuple-element.242) | copy-start | bytes 40
  54.5 42.5 %copy-start.24 = (u32[32]{0:T(128)S(1)}, u32[32]{0:T(128)}, u32[]{:S(2)}) copy-start(u32[32]{0:T(128)} %constant.117) | copy-start | bytes 388
  58.5 62.2 %copy-start = (f32[4,128,2]{2,1,0:T(8,128)}, f32[4,128,2]{2,1,0:T(8,128)S(1)}, u32[]{:S(2)}) copy-start(f32[4,128,2]{2,1,0:T(8,128)S(1)} %reduce_window_sum.45) | copy-start | bytes 12292
  60.1 60.7 %copy-start.5 = (bf16[512,3,64]{0,2,1:T(8,128)(2,1)S(1)}, bf16[512,3,64]{0,2,1:T(8,128)(2,1)}, u32[]{:S(2)}) copy-start(bf16[512,3,64]{0,2,1:T(8,128)(2,1)} %get-tuple-element.228) | copy-start | bytes 589828
  60.3 62.3 %copy-start.4 = (bf16[512,3,64]{0,2,1:T(8,128)(2,1)S(1)}, bf16[512,3,64]{0,2,1:T(8,128)(2,1)}, u32[]{:S(2)}) copy-start(bf16[512,3,64]{0,2,1:T(8,128)(2,1)} %get-tuple-element.229) | copy-start | bytes 589828
  129.6 11.1 %copy-start.1 = (f32[4,128,2]{2,1,0:T(8,128)S(1)}, f32[4,128,2]{2,1,0:T(8,128)}, u32[]{:S(2)}) copy-start(f32[4,128,2]{2,1,0:T(8,128)} %copy-done) | copy-start | bytes 12292
  132.8 7.5 %copy-start.17 = (f32[4,1,2]{0,2,1:T(2,128)S(1)}, f32[4,1,2]{0,2,1:T(2,128)}, u32[]{:S(2)}) copy-start(f32[4,1,2]{0,2,1:T(2,128)} %copy-done.16) | copy-start | bytes 100
  132.8 7.7 %copy-start.2 = (f32[4,128,2]{2,1,0:T(8,128)S(1)}, f32[4,128,2]{2,1,0:T(8,128)}, u32[]{:S(2)}) copy-start(f32[4,128,2]{2,1,0:T(8,128)} %get-tuple-element.236) | copy-start | bytes 12292
  132.8 8.1 %copy-start.11 = (bf16[2,4,4,8,128]{4,3,2,1,0:T(8,128)(2,1)S(1)}, bf16[2,4,4,8,128]{4,3,2,1,0:T(8,128)(2,1)}, u32[]{:S(2)}) copy-start(bf16[2,4,4,8,128]{4,3,2,1,0:T(8,128)(2,1)} %get-tuple-element.233) | copy-start | bytes 196612
  132.8 8.1 %copy-start.10 = (bf16[2,4,4,8,128]{4,3,2,1,0:T(8,128)(2,1)S(1)}, bf16[2,4,4,8,128]{4,3,2,1,0:T(8,128)(2,1)}, u32[]{:S(2)}) copy-start(bf16[2,4,4,8,128]{4,3,2,1,0:T(8,128)(2,1)} %get-tuple-element.232) | copy-start | bytes 196612
  132.8 8.1 %copy-start.12 = (f32[4,2,64,64]{3,2,1,0:T(8,128)S(1)}, f32[4,2,64,64]{3,2,1,0:T(8,128)}, u32[]{:S(2)}) copy-start(f32[4,2,64,64]{3,2,1,0:T(8,128)} %get-tuple-element.136) | copy-start | bytes 393220
  132.8 8.4 %copy-start.6 = (f32[4,128,2,64]{1,3,2,0:T(8,128)S(1)}, f32[4,128,2,64]{1,3,2,0:T(8,128)}, u32[]{:S(2)}) copy-start(f32[4,128,2,64]{1,3,2,0:T(8,128)} %bitcast_dynamic-update-slice_fusion.2) | copy-start | bytes 786436
  132.8 8.4 %copy-start.15 = (pred[128,128]{1,0:T(8,128)(4,1)S(1)}, pred[128,128]{1,0:T(8,128)(4,1)}, u32[]{:S(2)}) copy-start(pred[128,128]{1,0:T(8,128)(4,1)} %iota_compare_fusion) | copy-start | bytes 49156
  132.8 9.1 %copy-start.14 = (bf16[512,128]{1,0:T(8,128)(2,1)S(1)}, bf16[512,128]{1,0:T(8,128)(2,1)}, u32[]{:S(2)}) copy-start(bf16[512,128]{1,0:T(8,128)(2,1)} %param.31) | copy-start | bytes 393220
  136.8 10.8 %all-to-all-start = ((bf16[4,128,384]{1,2,0:T(8,128)(2,1)}), bf16[4,128,384]{1,2,0:T(8,128)(2,1)S(1)}, u32[]{:S(2)}, u32[]{:S(2)}) async-start(bf16[4,128,384]{1,2,0:T(8,128)(2,1)} %copy_bitcast_fusion), calls=%async_computation | async-start | bytes 786432 | tf_op jit(solution)/shard_map/all_to_all | solution.py:160
  147.7 7.9 %all-to-all-start.1 = ((bf16[4,128,128]{1,2,0:T(8,128)(2,1)}), bf16[4,128,128]{1,2,0:T(8,128)(2,1)S(1)}, u32[]{:S(2)}, u32[]{:S(2)}) async-start(bf16[4,128,128]{1,2,0:T(8,128)(2,1)} %copy_bitcast_fusion.1), calls=%async_computation.1 | async-start | bytes 262144 | tf_op jit(solution)/shard_map/all_to_all | solution.py:161
  151.0 35.0 %all-gather.13.cloned.1.call-start = ((), (), s32[]{:S(2)}) async-start(), calls=%async_computation.6 | async-start | bytes 2621440 | tf_op jit(solution)/shard_map/all_gather | solution.py:172
  155.0 2.7 copy-start.7
  155.1 2.7 copy-start.18
  155.1 3.0 copy-start.19
  155.1 4.0 copy-start.3
  164.1 293.2 %all-to-all-start.2 = ((bf16[8,2048,256]{1,2,0:T(8,128)(2,1)}), bf16[8,2048,256]{1,2,0:T(8,128)(2,1)}, u32[]{:S(2)}, u32[]{:S(2)}) async-start(bf16[8,2048,256]{1,2,0:T(8,128)(2,1)} %stack.2), calls=%async_computation.2 | async-start | bytes 16777216 | tf_op jit(solution)/shard_map/all_to_all | solution.py:184
  172.9 284.5 %all-gather.15.cloned.1.call-start = ((), (), s32[]{:S(2)}) async-start(), calls=%async_computation.7 | async-start | bytes 9437184 | tf_op jit(solution)/shard_map/all_gather | solution.py:176
  173.4 330.8 %reduce-scatter.2.cloned.1.call-start = ((), (), s32[]{:S(2)}) async-start(), calls=%async_computation.8 | async-start | bytes 2621440 | tf_op jit(solution)/shard_map/reduce_scatter | solution.py:188
  457.3 48.1 %copy-start.20 = (f32[2048]{0:T(1024)S(1)}, f32[2048]{0:T(1024)}, u32[]{:S(2)}) copy-start(f32[2048]{0:T(1024)} %param.41) | copy-start | bytes 24580
  (1 other events, 0.6 us)
Sparse Core Ops, SparseCore 0:
  8.9 49.1 all-gather.8
  59.6 22.5 all-gather.10
  159.2 26.6 all-gather.12
  187.9 259.5 all-gather.14
  474.0 30.1 reduce-scatter.1
